TPU v7x, 256 devices: a 4x2x16 block of a 4x16x16 slice. The times are simulated.
256 devices in a mesh: grp: 2 (over y), sp: 16 (over z), tp: 8 (over x, core).
Axes of the slice: x: 4, y: 2, z: 16, core: 2. Of those that a mesh axis runs over, the one named last changes fastest.
The devices are a block of a 4x16x16 slice.
Arguments:
- stream: bfloat16 [98304, 4096], P(('grp', 'sp', 'tp')), parts along dimension 0, may hold values from -6 to 6
- norm_gain: float32 [2, 4096], replicated, may hold values from 0.1 to 1.9
- mix_weight: bfloat16 [2, 4, 1024, 1024], P(None, None, 'sp', 'tp'), may hold values from -0.1875 to 0.1875
- branch_scale: float32 [2, 4096], replicated, may hold values from 0.1 to 1.9
Outputs:
- result: bfloat16 [98304, 4096], P(('grp', 'sp', 'tp')), parts along dimension 0
There are 2 independent parts, one for each index of `grp`. A program takes and returns all parts, laid end to end along the dimension named above; an argument that names none is the same for every part. Nothing has to cross between parts.
All inputs are finite; a program needn't handle non-finite values.
Results may differ from a plain program's by a relative error of at most 0.0056.
Values may be sent and summed in bfloat16 or wider, within the bound.
No kernel may reach another device: no remote copies, remote signals or barrier semaphores. Data moves between devices by JAX's collectives and lax.ppermute only.
A program may use at most 128 MiB of HBM per device.

v0:
```python
import jax
import jax.numpy as jnp
from jax import lax
from jax.sharding import PartitionSpec as P

GW = 1024
G = 4
LAYERS = 2


epsilon = 1e-06
window_lengths = (2, 4, 8, 16)
halo_rows = 15


def from_behind(block, axis, distance):
    devices = range(lax.axis_size(axis))
    route = [(i - distance, i) for i in devices if i - distance in devices]
    return lax.ppermute(block, axis, route)


def joined_along(pieces, dim):
    pieces = jnp.moveaxis(pieces, 0, dim)
    lengths = pieces.shape
    return pieces.reshape(*lengths[:dim], lengths[dim] * lengths[dim + 1], *lengths[dim + 2 :])


def sent_to_all(x, axis):
    length = lax.axis_size(axis)
    return lax.all_to_all(jnp.broadcast_to(x[None], (length, *x.shape)), axis, 0, 0, tiled=True)


def collect(x, axis, dim):
    return joined_along(sent_to_all(x, axis), dim)


def per_device(stream, norm_gain, mix_weight, branch_scale):
    row_count = stream.shape[0]
    feature_width = stream.shape[1]
    offset = lax.axis_index(("sp", "tp")) * row_count
    counts_base = (offset + lax.iota(jnp.int32, row_count)).astype(jnp.float32) + 1.0
    residual = stream.astype(jnp.float32)
    for layer_idx in range(LAYERS):
        scale_rows = lax.rsqrt(jnp.mean(residual * residual, axis=1, keepdims=True) + epsilon)
        normed = (residual * scale_rows * norm_gain[layer_idx]).astype(jnp.bfloat16)
        earlier = from_behind(normed[row_count - halo_rows :], ("sp", "tp"), 1)
        extended = jnp.concatenate([earlier, normed], axis=0).astype(jnp.float32)
        pieces = []
        for group_idx in range(G):
            window_len = window_lengths[group_idx]
            segment = extended[:, group_idx * GW : (group_idx + 1) * GW]
            own_rows = segment[halo_rows:]
            running = own_rows
            for back_step in range(1, window_len):
                running = (
                    running + segment[halo_rows - back_step : halo_rows - back_step + row_count]
                )
            window_mean = running / jnp.minimum(counts_base, float(window_len))[:, None]
            pieces.append((window_mean - own_rows).astype(jnp.bfloat16))
        pooled = jnp.stack(pieces, axis=1)
        weight_shard = mix_weight[layer_idx]
        full_rows = collect(weight_shard, "sp", 1)
        mixed_out = jnp.einsum(
            "rgc,gcn->rgn",
            pooled,
            lax.all_gather(full_rows, "tp", axis=2, tiled=True),
            preferred_element_type=jnp.float32,
        )
        residual = residual + mixed_out.reshape(row_count, feature_width) * branch_scale[layer_idx]
    return residual.astype(jnp.bfloat16)


def solution(mesh):
    return jax.shard_map(
        per_device,
        mesh=mesh,
        in_specs=(P(("grp", "sp", "tp"), None), P(), P(None, None, "sp", "tp"), P()),
        out_specs=P(("grp", "sp", "tp"), None),
        check_vma=False,
    )
```

profile of v0, /device:TPU:33, one launch (start us, length us, event | category | flops | bytes accessed | tf_op | source)
XLA Modules:
  0.0 229.3 jit_solution(12822001037860567513)
XLA Ops:
  7.7 69.6 %all_to_all.10 = bf16[16,4,64,128]{3,2,1,0:T(8,128)(2,1)S(1)} all-to-all(bf16[16,4,64,128]{3,2,1,0:T(8,128)(2,1)S(1)} %broadcast_in_dim.9), channel_id=1, replica_groups=mesh['grp'=2,'sp'=16,'tp'=8] {'sp'}, dimensions={0} | all-to-all | bytes 2097152 | tf_op jit(solution)/shard_map/all_to_all | solution.py:30
  77.2 1.1 copy.7
  78.7 57.7 %all_to_all.11 = bf16[16,4,64,128]{3,2,1,0:T(8,128)(2,1)S(1)} all-to-all(bf16[16,4,64,128]{3,2,1,0:T(8,128)(2,1)S(1)} %broadcast_in_dim.11), channel_id=1, replica_groups=mesh['grp'=2,'sp'=16,'tp'=8] {'sp'}, dimensions={0} | all-to-all | bytes 2097152 | tf_op jit(solution)/shard_map/all_to_all | solution.py:30
  136.5 1.1 copy.9
  137.6 1.2 copy-done.1
  139.6 1.0 fusion.2
  140.7 1.7 copy-done.2
  142.3 10.3 %collective-permute-start = (bf16[15,4096]{1,0:T(8,128)(2,1)S(1)}, bf16[15,4096]{1,0:T(8,128)(2,1)S(1)}, u32[]{:S(2)}, u32[]{:S(2)}) collective-permute-start(bf16[15,4096]{1,0:T(8,128)(2,1)S(1)} %slice.340), channel_id=1, source_target_pairs={{0,1},{1,2},{2,3},{3,4},{4,5},{5,6},{6,7},{7,8},{8,9},{9,10},{10,1... | collective-permute-start | bytes 368648 | tf_op jit(solution)/shard_map/ppermute | solution.py:19
  152.8 1.7 collective-permute-done
  154.4 2.8 %maximum_convert_fusion = f32[399,4096]{1,0:T(8,128)S(1)} fusion(bf16[384,4096]{1,0:T(8,128)(2,1)} %copy-done.2, bf16[15,4096]{1,0:T(8,128)(2,1)S(1)} %collective-permute-done), kind=kLoop, calls=%fused_computation.9 | loop fusion | flops 6537216 | bytes 9805824 | tf_op jit(solution)/shard_map/convert_element_type | solution.py:47
  157.3 3.3 %fusion.56 = bf16[384,1,1024]{2,0,1:T(8,128)(2,1)} fusion(f32[384]{0:T(512)S(1)} %fusion.57, f32[399,4096]{1,0:T(8,128)S(1)} %maximum_convert_fusion), kind=kLoop, calls=%fused_computation.112 | loop fusion | flops 7077888 | bytes 25953792 | tf_op jit(solution)/shard_map/stack | solution.py:60
  160.6 3.5 %fusion.50 = (bf16[384,1,1024]{2,0,1:T(8,128)(2,1)}, bf16[384,1,1024]{2,0,1:T(8,128)(2,1)}, bf16[384,1,1024]{2,0,1:T(8,128)(2,1)}) fusion(f32[384]{0:T(512)S(1)} %fusion.60, f32[399,4096]{1,0:T(8,128)S(1)} %maximum_convert_fusion, f32[384]{0:T(512)S(1)} %get-tuple-element.18, f32[384]{0:T(512)S(1)} %get-tuple-element.17), kind=kLoop, calls=%fused_computation.106 | loop fusion | flops 7864320 | bytes 24384000 | tf_op jit(solution)/shard_map/stack | solution.py:60
  164.1 7.9 %fusion.22 = f32[4,48,8,1024]{3,2,1,0:T(8,128)S(1)} fusion(bf16[4,1024,1024]{2,1,0:T(8,128)(2,1)} %all-gather.3.cloned.1.call-done, bf16[384,1,1024]{2,0,1:T(8,128)(2,1)} %fusion.56, bf16[384,1,1024]{2,0,1:T(8,128)(2,1)} %get-tuple-element.10, bf16[384,1,1024]{2,0,1:T(8,128)(2,1)} %get-tuple-element.9, bf16[384,1,1024]{2,0,1:T(8,128)(2,1)} %get-tuple-element.8), kind=kOutput, calls=%fused_computation.28 | convolution fusion | flops 3225944064 | bytes 17825792 | tf_op jit(solution)/shard_map/rgc,gcn->rgn/dot_general | solution.py:63
  172.6 1.2 multiply_reduce_fusion
  173.8 1.4 copy-done
  175.3 1.6 multiply_convert_fusion
  176.9 4.6 %collective-permute-start.1 = (bf16[15,4096]{1,0:T(8,128)(2,1)S(1)}, bf16[15,4096]{1,0:T(8,128)(2,1)S(1)}, u32[]{:S(2)}, u32[]{:S(2)}) collective-permute-start(bf16[15,4096]{1,0:T(8,128)(2,1)S(1)} %slice.371), channel_id=1, source_target_pairs={{0,1},{1,2},{2,3},{3,4},{4,5},{5,6},{6,7},{7,8},{8,9},{9,10},{10,1... | collective-permute-start | bytes 368648 | tf_op jit(solution)/shard_map/ppermute | solution.py:19
  181.5 4.6 %collective-permute-done.1 = bf16[15,4096]{1,0:T(8,128)(2,1)S(1)} collective-permute-done((bf16[15,4096]{1,0:T(8,128)(2,1)S(1)}, bf16[15,4096]{1,0:T(8,128)(2,1)S(1)}, u32[]{:S(2)}, u32[]{:S(2)}) %collective-permute-start.1) | collective-permute-done | bytes 122912 | tf_op jit(solution)/shard_map/ppermute | solution.py:19
  187.0 3.3 %fusion.55 = bf16[384,1,1024]{2,0,1:T(8,128)(2,1)} fusion(f32[384]{0:T(512)S(1)} %fusion.57, f32[399,4096]{1,0:T(8,128)S(1)} %maximum_convert_fusion.1), kind=kLoop, calls=%fused_computation.111 | loop fusion | flops 7077888 | bytes 25953792 | tf_op jit(solution)/shard_map/stack | solution.py:60
  190.2 3.5 %fusion.49 = (bf16[384,1,1024]{2,0,1:T(8,128)(2,1)}, bf16[384,1,1024]{2,0,1:T(8,128)(2,1)}, bf16[384,1,1024]{2,0,1:T(8,128)(2,1)}) fusion(f32[384]{0:T(512)S(1)} %fusion.60, f32[399,4096]{1,0:T(8,128)S(1)} %maximum_convert_fusion.1, f32[384]{0:T(512)S(1)} %get-tuple-element.18, f32[384]{0:T(512)S(1)} %get-tuple-element.17), kind=kLoop, calls=%fused_computation.105 | loop fusion | flops 7864320 | bytes 24384000 | tf_op jit(solution)/shard_map/stack | solution.py:60
  193.8 11.1 %all-gather.5.cloned.1.call-done = bf16[4,1024,1024]{2,1,0:T(8,128)(2,1)} async-done(((bf16[4,1024,128]{2,1,0:T(8,128)(2,1)}), bf16[4,1024,1024]{2,1,0:T(8,128)(2,1)}) %all-gather.5.cloned.1.call-update) | async-done | bytes 8388624 | tf_op jit(solution)/shard_map/all_gather | solution.py:66
  204.9 7.9 %fusion.19 = f32[4,48,8,1024]{3,2,1,0:T(8,128)S(1)} fusion(bf16[4,1024,1024]{2,1,0:T(8,128)(2,1)} %all-gather.5.cloned.1.call-done, bf16[384,1,1024]{2,0,1:T(8,128)(2,1)} %fusion.55, bf16[384,1,1024]{2,0,1:T(8,128)(2,1)} %get-tuple-element.7, bf16[384,1,1024]{2,0,1:T(8,128)(2,1)} %get-tuple-element.6, bf16[384,1,1024]{2,0,1:T(8,128)(2,1)} %get-tuple-element.5), kind=kOutput, calls=%fused_computation.27 | convolution fusion | flops 3225944064 | bytes 17825792 | tf_op jit(solution)/shard_map/rgc,gcn->rgn/dot_general | solution.py:63
  212.8 3.4 %copy.12 = f32[4,48,8,1024]{3,2,0,1:T(8,128)} copy(f32[4,48,8,1024]{3,2,1,0:T(8,128)S(1)} %fusion.19) | data formatting | bytes 12582912 | tf_op jit(solution)/shard_map/reshape | solution.py:69
  216.2 6.2 %add_convert_fusion = bf16[384,4096]{1,0:T(8,128)(2,1)} fusion(f32[384,4096]{1,0:T(8,128)} %bitcast.43, f32[4096]{0:T(1024)S(1)} %bitcast.51, f32[384,4096]{1,0:T(8,128)S(1)} %bitcast.42, f32[4096]{0:T(1024)S(1)} %bitcast.50, bf16[384,4096]{1,0:T(8,128)(2,1)S(1)} %copy-done.1), kind=kLoop, calls=%fused_computation.6 | loop fusion | flops 9437184 | bytes 18907136 | tf_op jit(solution)/shard_map/convert_element_type | solution.py:70
  (32 shorter events, 4.0 us)
Async XLA Ops:
  6.5 157.6 %all-gather.3.cloned.1.call-start = ((), (), s32[]{:S(2)}) async-start(), calls=%async_computation.2 | async-start | bytes 9437184 | tf_op jit(solution)/shard_map/all_gather | solution.py:66
  78.4 126.5 %all-gather.5.cloned.1.call-start = ((), (), s32[]{:S(2)}) async-start(), calls=%async_computation.3 | async-start | bytes 9437184 | tf_op jit(solution)/shard_map/all_gather | solution.py:66
  136.5 2.4 %copy-start.1 = (bf16[384,4096]{1,0:T(8,128)(2,1)S(1)}, bf16[384,4096]{1,0:T(8,128)(2,1)}, u32[]{:S(2)}) copy-start(bf16[384,4096]{1,0:T(8,128)(2,1)} %param.4) | copy-start | bytes 9437188
  138.8 0.8 copy-start.3
  139.6 13.1 %copy-start.4 = (f32[2,4096]{1,0:T(2,128)S(1)}, f32[2,4096]{1,0:T(2,128)}, u32[]{:S(2)}) copy-start(f32[2,4096]{1,0:T(2,128)} %param.7) | copy-start | bytes 98308
  140.6 1.7 copy-start.2
  142.3 12.1 %collective-permute-start = (bf16[15,4096]{1,0:T(8,128)(2,1)S(1)}, bf16[15,4096]{1,0:T(8,128)(2,1)S(1)}, u32[]{:S(2)}, u32[]{:S(2)}) collective-permute-start(bf16[15,4096]{1,0:T(8,128)(2,1)S(1)} %slice.340), channel_id=1, source_target_pairs={{0,1},{1,2},{2,3},{3,4},{4,5},{5,6},{6,7},{7,8},{8,9},{9,10},{10,1... | collective-permute-start | bytes 368648 | tf_op jit(solution)/shard_map/ppermute | solution.py:19
  172.6 2.7 %copy-start = (f32[4,48,8,1024]{3,2,0,1:T(8,128)}, f32[4,48,8,1024]{3,2,0,1:T(8,128)S(1)}, u32[]{:S(2)}) copy-start(f32[4,48,8,1024]{3,2,0,1:T(8,128)S(1)} %copy.11) | copy-start | bytes 18874372
  176.9 9.2 %collective-permute-start.1 = (bf16[15,4096]{1,0:T(8,128)(2,1)S(1)}, bf16[15,4096]{1,0:T(8,128)(2,1)S(1)}, u32[]{:S(2)}, u32[]{:S(2)}) collective-permute-start(bf16[15,4096]{1,0:T(8,128)(2,1)S(1)} %slice.371), channel_id=1, source_target_pairs={{0,1},{1,2},{2,3},{3,4},{4,5},{5,6},{6,7},{7,8},{8,9},{9,10},{10,1... | collective-permute-start | bytes 368648 | tf_op jit(solution)/shard_map/ppermute | solution.py:19
  204.9 11.3 %slice-start = ((s8[6291456]{0:T(1024)(128)(4,1)}), s8[4194304]{0:T(1024)(128)(4,1)S(1)}, s32[]{:S(2)}) async-start(s8[6291456]{0:T(1024)(128)(4,1)} %bitcast.40), calls=%async_computation.4 | async-start | bytes 8388608
  204.9 11.3 %slice-start.1 = ((s8[6291456]{0:T(1024)(128)(4,1)}), s8[2097152]{0:T(1024)(128)(4,1)S(1)}, s32[]{:S(2)}) async-start(s8[6291456]{0:T(1024)(128)(4,1)} %bitcast.40), calls=%async_computation.5 | async-start | bytes 4194304
Sparse Core Ops, SparseCore 0:
  78.5 62.6 all-gather.2
  143.1 61.7 all-gather.4
where the time goes:
time: 230 us; the launch traced here: 229 us
  blocking collectives  127 us (55%)
  other arithmetic  28.1 us (12%)
  waiting for transfers between devices  17.5 us (8%)
  matrix products  15.8 us (7%)
  starting transfers between devices  15 us (7%)
  between operations  13.6 us (6%)
  local copies, waits for them, and re-layouts  12.1 us (5%)
    all_to_all x2, blocking collectives, sent_to_all(): lax.all_to_all(jnp.broadcast_to(x[None], (length, *x.shape)), axis, 0, 0,...  127 us
    dot_general x2, matrix products, per_device(): jnp.einsum('rgc,gcn->rgn', pooled, lax.all_gather(full_rows, 'tp', axis=2...  15.8 us
    ppermute x2, starting transfers between devices, from_behind(): return lax.ppermute(block, axis, route)  14.9 us
    another operation x4, other arithmetic, per_device(): pooled = jnp.stack(pieces, axis=1)  13.6 us
    all_gather x2, waiting for transfers between devices, per_device(): lax.all_gather(full_rows, 'tp', axis=2, tiled=True)  11.1 us
    ppermute x2, waiting for transfers between devices, from_behind(): return lax.ppermute(block, axis, route)  6.25 us
    convert_element_type x1, other arithmetic, per_device(): return residual.astype(jnp.bfloat16)  6.2 us
  transfers between devices with their start and end apart: 4, of which 3 were waited for; matrix products, arithmetic and copies ran while one was open for 14% of the time, Pallas kernels for 0%

commit v1 on v0

v1 whole, which is shorter than its diff:
```python
import functools

import jax
import jax.numpy as jnp
from jax import lax
from jax.experimental import pallas as pl
from jax.experimental.pallas import tpu as pltpu
from jax.sharding import PartitionSpec as P


GW = 1024
G = 4
D = G * GW
EPS = 1e-06
WINDOWS = (2, 4, 8, 16)
HALO = 16
LAYERS = 2
CORES = 2
NZ = 16
NX = 4


OFFSETS = (4, 0, -4, -8, 3, -1, -5, -9, 5, 1, -3, -7, -2, -6, 6, 2)
SHARED = (0,)
COMMON = 2

CHIPS = (("h", 0), ("o", 2), ("l", 3), ("r", 1))


def issued(v, axis, route):
    n = lax.axis_size(axis)
    return lax.ppermute(v, axis, [(i, route(i, n)) for i in range(n)])


def shift_sp(v, distance):
    return issued(v, "sp", lambda i, n: (i + distance) % n)


def shift_x(v, distance):
    return issued(v, "tp", lambda i, n: (i + CORES * distance) % n)


def swap_core(v):
    return issued(v, "tp", lambda i, n: i ^ 1)


def swap_grp(v):
    return issued(v, "grp", lambda i, n: i ^ 1)


def join(layout, *arrays):
    shapes = []
    for out in layout:
        parts = [jax.eval_shape(lambda v, cut=cut: cut(v), arrays[i]) for i, cut in out]
        shapes.append(jax.ShapeDtypeStruct((sum(p.shape[0] for p in parts), *parts[0].shape[1:]), parts[0].dtype))

    def body(*refs):
        for out, ref in zip(layout, refs[len(arrays) :]):
            at = 0
            for i, cut in out:
                v = cut(refs[i])
                ref[at : at + v.shape[0]] = v
                at += v.shape[0]

    out = pl.pallas_call(
        body, out_shape=tuple(shapes), in_specs=[VMEM] * len(arrays), out_specs=tuple(VMEM for _ in shapes)
    )(*arrays)
    return out


def take(*index):
    return lambda v: v[index if len(index) > 1 else index[0]]


VMEM = pl.BlockSpec(memory_space=pltpu.VMEM)
HBM = pl.BlockSpec(memory_space=pltpu.HBM)
MIB = 1024 * 1024


def gather(piece):
    up, down, far = shift_sp(piece, 4), shift_sp(piece, -4), shift_sp(piece, 8)
    sets = join(
        [
            [(i, take(slice(layer, layer + 1))) for i in places]
            for layer in range(LAYERS)
            for places in ((0, 1, 2, 3), (1, 2), (0, 1))
        ],
        down, piece, up, far,
    )
    layers = []
    for layer in range(LAYERS):
        s, s1, s2 = sets[3 * layer : 3 * layer + 3]
        near = [s] + [shift_sp(v, d) for v, d in ((s, 1), (s, -1), (s1, 2), (s2, -2))]
        shared = layer in SHARED
        home, mine, *cut = join_halves(shared, *near)
        opposite = shift_x(mine, 2)
        own = {"h": home, "o": opposite, "yo": swap_grp(opposite)}
        for name, distance in (("l", 1), ("r", -1)):
            if shared:
                common, half = cut
                half = shift_x(half, distance)
                own |= {name + "c": shift_x(common, distance), name + "e": half}
                own["y" + name + "e"] = swap_grp(half)
            else:
                own[name] = shift_x(home, distance)
        theirs = {n: swap_core(v) for n, v in own.items()}
        layers.append((tuple(own), [*own.values(), *theirs.values()]))
    return layers


def join_halves(shared, *arrays):
    n = sum(v.shape[0] for v in arrays)
    slots, rest = arrays[0].shape[1], arrays[0].shape[2:]

    def body(*refs):
        whole, mine, *cut = refs[len(arrays) :]
        at = 0
        for r in refs[: len(arrays)]:
            whole[at : at + r.shape[0]] = r[...]
            at += r.shape[0]
        mine[...] = whole[pl.ds((lax.axis_index("grp") % 2) * (n // 2), n // 2)]
        if shared:
            cut[0][...] = whole[:, :COMMON]
            cut[1][...] = mine[:, COMMON:]

    sizes = [(n, slots), (n // 2, slots)] + [(n, COMMON), (n // 2, slots - COMMON)] * shared
    shapes = tuple(jax.ShapeDtypeStruct((*m, *rest), arrays[0].dtype) for m in sizes)
    return pl.pallas_call(
        body, out_shape=shapes, in_specs=[VMEM] * len(arrays), out_specs=(VMEM,) * len(shapes)
    )(*arrays)


def position():
    tp = lax.axis_index("tp")
    return lax.axis_index("sp"), tp // CORES, tp % CORES


def first_row(rows):
    return (lax.axis_index("sp") * lax.axis_size("tp") + lax.axis_index("tp")) * rows


def norm_rows(load, gain_ref, n_ref, base, rows):
    def step(i, _):
        r = pl.multiple_of(i * 16, 16)
        v = load(r)
        scale = lax.rsqrt(jnp.sum(v * v, axis=1, keepdims=True) * (1.0 / D) + EPS)
        n_ref[pl.ds(base + r, 16), :] = (v * scale * gain_ref[0:1, :]).astype(jnp.bfloat16)
        return 0

    lax.fori_loop(0, rows // 16, step, 0, unroll=2)


def pool_rows(get, out_ref, rows, block, first):
    sp = position()[0]
    chunk = sp // 2
    odd = jnp.full((block, 128), sp % 2, jnp.int32) == 1
    low = lax.broadcasted_iota(jnp.int32, (block, 128), 1) < 64
    for g, window in enumerate(WINDOWS):

        def step(i, _, g=g, window=window):
            r = pl.multiple_of(i * block, 16)
            pos = first + r + lax.broadcasted_iota(jnp.int32, (block, 1), 0)
            inv = 1.0 / jnp.clip(pos + 1, 1, window).astype(jnp.float32)
            plain, turned = [], []
            for t in range(8):
                c = pl.multiple_of(g * GW + ((chunk + t) % 8) * 128, 128)
                v = get(r, block + HALO, c)
                s, d = v, 1
                while d < window:
                    s = s + pltpu.roll(s, d, 0)
                    d *= 2
                p = s[HALO:] * inv - v[HALO:]
                plain.append(p)
                turned.append(pltpu.roll(p, 64, 1))
            for t in range(8):
                o = jnp.where(odd, jnp.where(low, turned[t], turned[(t + 1) % 8]), plain[t])
                out_ref[pl.ds(r, block), g * GW + t * 128 : g * GW + (t + 1) * 128] = o.astype(jnp.bfloat16)
            return 0

        lax.fori_loop(0, rows // block, step, 0)


def fetch(names, parts, buffers, sems):
    waits = {n: [] for n in names}
    for i, (part, buffer) in enumerate(zip(parts, buffers)):
        copy = pltpu.make_async_copy(part, buffer, sems.at[i])
        copy.start()
        waits[names[i % len(names)]].append(copy)
    return waits


def mix(pooled_ref, names, buffers, waits, emit, start=None, finish=None, unroll=False):
    place = {o % NZ: k for k, o in enumerate(OFFSETS)}
    half = NZ // 2
    _, chip, own = position()
    odd = jnp.full((GW // NZ, 128), lax.axis_index("grp") % 2, jnp.int32) == 1
    held = [dict(zip(names, buffers[dc * len(names) :])) for dc in range(CORES)]

    def weight(name, dc, g, k, common):
        refs = held[dc]
        if name + "c" in refs:
            if common:
                return refs[name + "c"][k, g]
            name, g = name + "e", g - COMMON
        if "y" + name not in refs:
            return refs[name][k, g]
        brought, peers = refs[name][k % half, g], refs["y" + name][k % half, g]
        return jnp.where(odd, peers, brought) if k < half else jnp.where(odd, brought, peers)

    for name, dx in CHIPS:
        if not any(name in n for n in names):
            continue
        for n in names:
            if name in n:
                for copy in waits[n]:
                    copy.wait()
        if start:
            start(name)
        x = (chip + dx) % NX

        def group(g, common, name=name, x=x):
            cols = [jnp.concatenate([weight(name, dc, g, place[j], common) for j in range(NZ)], axis=0) for dc in range(CORES)]
            lhs = pooled_ref[:, pl.ds(pl.multiple_of(g * GW, GW), GW)]
            m = jnp.dot(lhs, jnp.concatenate(cols, axis=1), preferred_element_type=jnp.float32)
            at = pl.multiple_of(g * GW + x * 256, 256)
            emit(name, g, at, [(pl.multiple_of((own + dc) % CORES * 128, 128), m[:, dc * 128 : (dc + 1) * 128]) for dc in range(CORES)])

        for lo, hi in ((0, COMMON), (COMMON, G)) if name + "c" in names else ((0, G),):
            if unroll:
                for g in range(lo, hi):
                    group(g, hi == COMMON)
            else:
                lax.fori_loop(lo, hi, lambda g, _: group(g, hi == COMMON), None)
        if finish:
            finish(name)


def pool_kernel(halo_ref, gain_ref, stream_hbm, out_hbm, stream_ref, out_ref, n_ref, sems):
    rows = stream_ref.shape[0]
    read = pltpu.make_async_copy(stream_hbm, stream_ref, sems.at[0])
    read.start()
    norm_rows(lambda r: halo_ref[pl.ds(r, 16), :].astype(jnp.float32), gain_ref, n_ref, 0, 2 * HALO)
    read.wait()
    norm_rows(lambda r: stream_ref[pl.ds(r, 16), :].astype(jnp.float32), gain_ref, n_ref, 2 * HALO, rows)
    pool_rows(
        lambda r, n, c: n_ref[pl.ds(r, n), pl.ds(c, 128)].astype(jnp.float32), out_ref, rows + HALO, 80, first_row(rows) - HALO
    )
    write = pltpu.make_async_copy(out_ref, out_hbm, sems.at[1])
    write.start()
    write.wait()


def middle_kernel(names, halo_ref, stream_ref, pooled_ref, scale_ref, gain_ref, *rest):
    n = CORES * len(names)
    parts, (res_out, pooled_out), (r_ref, square_ref, norm_ref, out_sems) = rest[:n], rest[n : n + 2], rest[n + 2 : n + 6]
    buffers, sems = rest[n + 6 : -1], rest[-1]
    waits = fetch(names, parts, buffers, sems)
    rows = stream_ref.shape[0]
    square_ref[...] = jnp.zeros_like(square_ref)
    copies = {}
    for i, (name, dx) in enumerate(CHIPS):
        at = [pl.multiple_of(g * GW + (position()[1] + dx) % NX * 256, 256) for g in range(G)]
        copies[name] = [
            pltpu.make_async_copy(r_ref.at[pl.ds(HALO, rows), pl.ds(c, 256)], res_out.at[:, pl.ds(c, 256)], out_sems.at[i * G + g])
            for g, c in enumerate(at)
        ]

    def emit(name, g, at, pieces):
        for shift, m in pieces:
            cols = pl.ds(at + shift, 128)
            m = m * scale_ref[0:1, cols]
            top = halo_ref[HALO:, cols].astype(jnp.float32) + m[:HALO]
            body = stream_ref[:, cols].astype(jnp.float32) + m[HALO:]
            r_ref[:HALO, cols] = top
            r_ref[HALO:, cols] = body
            square_ref[:HALO] += top * top
            square_ref[HALO:] += body * body

    def finish(name):
        for copy in copies[name]:
            copy.start()

    mix(pooled_ref, names, buffers, waits, emit, finish=finish, unroll=True)
    scale = lax.rsqrt(jnp.sum(square_ref[...], axis=1, keepdims=True) * (1.0 / D) + EPS)
    norm_ref[...] = jnp.broadcast_to(scale, norm_ref.shape)

    def get(r, n, c):
        cols = pl.ds(c, 128)
        v = r_ref[pl.ds(r, n), cols] * norm_ref[pl.ds(r, n), :] * gain_ref[1:2, cols]
        return v.astype(jnp.bfloat16).astype(jnp.float32)

    pool_rows(get, pooled_out, rows, 96, first_row(rows))
    for name, _ in CHIPS:
        for copy in copies[name]:
            copy.wait()


def last_kernel(names, res_ref, pooled_ref, scale_ref, *rest):
    n = CORES * len(names)
    parts, rest = rest[:n], rest[len(rest) - 5 - n :]
    out_ref, r_ref, o_ref, in_sems, out_sems = rest[0], rest[1], rest[2], rest[3], rest[4]
    buffers, sems = rest[5:], in_sems
    chip = position()[1]
    used = [(name, dx) for name, dx in CHIPS if any(name in n for n in names)]
    waits = fetch(names, parts, buffers, sems)
    reads, writes = [], []
    for i, (_, dx) in enumerate(used):
        for g in range(G):
            cols = pl.ds(pl.multiple_of(g * GW + (chip + dx) % NX * 256, 256), 256)
            k = i * G + g
            reads.append(pltpu.make_async_copy(res_ref.at[:, cols], r_ref.at[k], in_sems.at[n + k]))
            writes.append(pltpu.make_async_copy(o_ref.at[k], out_ref.at[:, cols], out_sems.at[k]))
    for copy in reads:
        copy.start()
    first = {name: i * G for i, (name, _) in enumerate(used)}

    def start(name):
        for copy in reads[first[name] : first[name] + G]:
            copy.wait()

    def finish(name):
        for copy in writes[first[name] : first[name] + G]:
            copy.start()

    def emit(name, g, at, pieces):
        k = first[name] + g
        for shift, m in pieces:
            cols = pl.ds(shift, 128)
            o_ref[k, :, cols] = (r_ref[k, :, cols] + m * scale_ref[1:2, pl.ds(at + shift, 128)]).astype(jnp.bfloat16)

    mix(pooled_ref, names, buffers, waits, emit, start, finish)
    for copy in writes:
        copy.wait()


def last_call(residual, pooled, scale, names, parts, before):
    rows = residual.shape[0]
    blocks = G * sum(any(c in n for n in names) for c, _ in CHIPS)
    more = [] if before is None else [before]
    return pl.pallas_call(
        functools.partial(last_kernel, names),
        out_shape=jax.ShapeDtypeStruct((rows, D), jnp.bfloat16),
        in_specs=[HBM, VMEM, VMEM] + [HBM] * (len(parts) + len(more)),
        out_specs=HBM,
        scratch_shapes=[
            pltpu.VMEM((blocks, rows, 256), jnp.float32),
            pltpu.VMEM((blocks, rows, 256), jnp.bfloat16),
            pltpu.SemaphoreType.DMA((len(parts) + blocks,)),
            pltpu.SemaphoreType.DMA((blocks,)),
        ]
        + [pltpu.VMEM(v.shape, v.dtype) for v in parts],
        input_output_aliases={3 + len(parts): 0} if more else {},
        compiler_params=pltpu.CompilerParams(vmem_limit_bytes=24 * MIB),
    )(residual, pooled, scale, *parts, *more)


def call(kernel, out_shape, out_specs, args, scratch, limit, names=(), parts=()):
    if names:
        kernel = functools.partial(kernel, names)
        scratch = scratch + [pltpu.VMEM(v.shape, v.dtype) for v in parts] + [pltpu.SemaphoreType.DMA((len(parts),))]
    return pl.pallas_call(
        kernel,
        out_shape=out_shape,
        in_specs=[VMEM] * len(args) + [HBM] * len(parts),
        out_specs=out_specs,
        scratch_shapes=scratch,
        compiler_params=pltpu.CompilerParams(vmem_limit_bytes=limit * MIB),
    )(*args, *parts)


def per_device(stream, norm_gain, mix_weight, branch_scale):
    rows = stream.shape[0]
    n = NZ * lax.axis_size("tp")
    tail = stream[rows - 2 * HALO :]
    halo = lax.ppermute(tail, ("sp", "tp"), [(i, i + 1) for i in range(n - 1)])
    w0, w1 = gather(mix_weight)
    bf, f32 = jnp.bfloat16, jnp.float32
    shape = jax.ShapeDtypeStruct
    pooled = call(
        pool_kernel, shape((rows + HALO, D), bf), HBM, (halo, norm_gain),
        [pltpu.VMEM((rows, D), bf), pltpu.VMEM((rows + HALO, D), bf), pltpu.VMEM((rows + 2 * HALO, D), bf),
         pltpu.SemaphoreType.DMA((2,))], 24, (), (stream,),
    )
    args = [halo, stream, pooled, branch_scale, norm_gain]
    ext = rows + HALO
    residual, pooled = call(
        middle_kernel, (shape((rows, D), f32), shape((rows, D), bf)), (HBM, VMEM), args,
        [pltpu.VMEM((ext, D), f32), pltpu.VMEM((ext, 128), f32), pltpu.VMEM((ext, 128), f32),
         pltpu.SemaphoreType.DMA((G * NX,))], 40, *w0,
    )
    names, parts = w1
    out = None
    for some in ("ho", "lr"):
        keep = [n for n in names if set(n) & set(some)]
        mine = [v for n, v in zip(names * CORES, parts) if n in keep]
        out = last_call(residual, pooled, branch_scale, tuple(keep), mine, out)
    return out


def solution(mesh):
    return jax.shard_map(
        per_device,
        mesh=mesh,
        in_specs=(P(("grp", "sp", "tp"), None), P(), P(None, None, "sp", "tp"), P()),
        out_specs=P(("grp", "sp", "tp"), None),
        check_vma=False,
    )
```

time: 230 us -> 204 us (0.89)
  blocking collectives: 127 us -> 0 us
  starting transfers between devices: 15 us -> 87.8 us
  waiting for transfers between devices: 17.5 us -> 69.8 us
  Pallas kernels: 0 us -> 37.7 us
  other arithmetic: 28.1 us -> 0 us
  matrix products: 15.8 us -> 0 us
  between operations: 13.6 us -> 0.35 us
  local copies, waits for them, and re-layouts: 12.1 us -> 8.23 us
    all_to_all x2 -> x0, blocking collectives: 127 us -> none  [sent_to_all(): lax.all_to_all(jnp.broadcast_to(x[None], (length, *x.shape)), axis, 0, 0,...]
    ppermute x2 -> x38, starting transfers between devices: 14.9 us -> 87.8 us  [the longest x37 80.7 us: issued(): return lax.ppermute(v, axis, [(i, route(i, n)) for i in range(n)])]
    ppermute x2 -> x38, waiting for transfers between devices: 6.25 us -> 69.8 us  [the longest x37 69.8 us: issued(): return lax.ppermute(v, axis, [(i, route(i, n)) for i in range(n)])]
    pallas_call x0 -> x7, Pallas kernels: none -> 37.7 us  [the longest x2 20.9 us: call(): pl.pallas_call(kernel, out_shape=out_shape, in_specs=[VMEM] * len(args) +...]
    dot_general x2 -> x0, matrix products: 15.8 us -> none  [per_device(): jnp.einsum('rgc,gcn->rgn', pooled, lax.all_gather(full_rows, 'tp', axis=2...]
    another operation x4 -> x0, other arithmetic: 13.6 us -> none  [per_device(): pooled = jnp.stack(pieces, axis=1)]
    convert_element_type x5 -> x0, other arithmetic: 12.5 us -> none  [the longest x1 6.2 us: per_device(): return residual.astype(jnp.bfloat16)]
    all_gather x2 -> x0, waiting for transfers between devices: 11.1 us -> none  [per_device(): lax.all_gather(full_rows, 'tp', axis=2, tiled=True)]
  transfers between devices with their start and end apart: 4 -> 38, of which waited for: 3 -> 11; matrix products, arithmetic and copies ran while one was open for 14% -> 1% of each run, Pallas kernels for 0% -> 15%
where the time goes in v1:
time: 204 us
  starting transfers between devices  87.8 us (43%)
  waiting for transfers between devices  69.8 us (34%)
  Pallas kernels  37.7 us (18%)
  local copies, waits for them, and re-layouts  8.23 us (4%)
    ppermute x37, starting transfers between devices, issued(): return lax.ppermute(v, axis, [(i, route(i, n)) for i in range(n)])  80.7 us
    ppermute x37, waiting for transfers between devices, issued(): return lax.ppermute(v, axis, [(i, route(i, n)) for i in range(n)])  69.8 us
    pallas_call x2, Pallas kernels, call(): pl.pallas_call(kernel, out_shape=out_shape, in_specs=[VMEM] * len(args) +...  20.9 us
    pallas_call x2, Pallas kernels, last_call(): pl.pallas_call(functools.partial(last_kernel, names), out_shape=jax.Shape...  9.49 us
    ppermute x1, starting transfers between devices, per_device(): halo = lax.ppermute(tail, ('sp', 'tp'), [(i, i + 1) for i in range(n - 1)])  7.16 us
    unnamed x26, local copies, waits for them, and re-layouts  6.57 us
    pallas_call x2, Pallas kernels, join_halves(): pl.pallas_call(body, out_shape=shapes, in_specs=[VMEM] * len(arrays), out...  5.12 us
  transfers between devices with their start and end apart: 38, of which 11 were waited for; matrix products, arithmetic and copies ran while one was open for 1% of the time, Pallas kernels for 15%

profile of v1, /device:TPU:33, one launch (start us, length us, event | category | flops | bytes accessed | tf_op | source)
XLA Modules:
  0.0 203.9 jit_solution(17410195028957544561)
XLA Ops:
  0.0 21.7 %collective-permute-start.1 = (bf16[2,4,64,128]{3,2,1,0:T(8,128)(2,1)}, bf16[2,4,64,128]{3,2,1,0:T(8,128)(2,1)S(1)}, u32[]{:S(2)}, u32[]{:S(2)}) collective-permute-start(bf16[2,4,64,128]{3,2,1,0:T(8,128)(2,1)} %refs_1_.1), channel_id=1, source_target_pairs={{0,96},{8,104},{16,112},{24,120},{32,0},{40,8},{48,16},{56,24},{64... | collective-permute-start | bytes 393224 | tf_op jit(solution)/shard_map/ppermute | solution.py:32
  21.7 5.2 %collective-permute-start.3 = (bf16[2,4,64,128]{3,2,1,0:T(8,128)(2,1)}, bf16[2,4,64,128]{3,2,1,0:T(8,128)(2,1)S(1)}, u32[]{:S(2)}, u32[]{:S(2)}) collective-permute-start(bf16[2,4,64,128]{3,2,1,0:T(8,128)(2,1)} %refs_1_.1), channel_id=1, source_target_pairs={{0,64},{8,72},{16,80},{24,88},{32,96},{40,104},{48,112},{56,120},{... | collective-permute-start | bytes 393224 | tf_op jit(solution)/shard_map/ppermute | solution.py:32
  26.9 6.8 %collective-permute-done.2.refs_2_ = bf16[2,4,64,128]{3,2,1,0:T(8,128)(2,1)S(1)} collective-permute-done((bf16[2,4,64,128]{3,2,1,0:T(8,128)(2,1)}, bf16[2,4,64,128]{3,2,1,0:T(8,128)(2,1)S(1)}, u32[]{:S(2)}, u32[]{:S(2)}) %collective-permute-start.2) | collective-permute-done | bytes 131104 | tf_op jit(solution)/shard_map/ppermute | solution.py:32
  33.7 13.9 %collective-permute-done.3.refs_3_ = bf16[2,4,64,128]{3,2,1,0:T(8,128)(2,1)S(1)} collective-permute-done((bf16[2,4,64,128]{3,2,1,0:T(8,128)(2,1)}, bf16[2,4,64,128]{3,2,1,0:T(8,128)(2,1)S(1)}, u32[]{:S(2)}, u32[]{:S(2)}) %collective-permute-start.3) | collective-permute-done | bytes 131104 | tf_op jit(solution)/shard_map/ppermute | solution.py:32
  50.4 2.7 %collective-permute-start.5 = (bf16[4,4,64,128]{3,2,1,0:T(8,128)(2,1)}, bf16[4,4,64,128]{3,2,1,0:T(8,128)(2,1)}, u32[]{:S(2)}, u32[]{:S(2)}) collective-permute-start(bf16[4,4,64,128]{3,2,1,0:T(8,128)(2,1)} %get-tuple-element.19.refs_0_), channel_id=1, source_target_pairs={{0,120},{8,0},{16,8},{24,16},{32,24},{40,32},{48,40},{56,48},{64,5... | collective-permute-start | bytes 786440 | tf_op jit(solution)/shard_map/ppermute | solution.py:32
  54.8 3.5 %collective-permute-start.7 = (bf16[2,4,64,128]{3,2,1,0:T(8,128)(2,1)}, bf16[2,4,64,128]{3,2,1,0:T(8,128)(2,1)}, u32[]{:S(2)}, u32[]{:S(2)}) collective-permute-start(bf16[2,4,64,128]{3,2,1,0:T(8,128)(2,1)} %get-tuple-element.21), channel_id=1, source_target_pairs={{0,112},{8,120},{16,0},{24,8},{32,16},{40,24},{48,32},{56,40},{64,... | collective-permute-start | bytes 393224 | tf_op jit(solution)/shard_map/ppermute | solution.py:32
  58.3 7.2 %collective-permute-start = (bf16[32,4096]{1,0:T(8,128)(2,1)}, bf16[32,4096]{1,0:T(8,128)(2,1)S(1)}, u32[]{:S(2)}, u32[]{:S(2)}) collective-permute-start(bf16[32,4096]{1,0:T(8,128)(2,1)} %slice.3), channel_id=1, source_target_pairs={{0,1},{1,2},{2,3},{3,4},{4,5},{5,6},{6,7},{7,8},{8,9},{9,10},{10,1... | collective-permute-start | bytes 786440 | tf_op jit(solution)/shard_map/ppermute | solution.py:375
  66.1 2.7 %shard_map.48 = (bf16[16,4,64,128]{3,2,1,0:T(8,128)(2,1)}, bf16[8,4,64,128]{3,2,1,0:T(8,128)(2,1)}, bf16[16,2,64,128]{3,2,1,0:T(8,128)(2,1)}, bf16[8,2,64,128]{3,2,1,0:T(8,128)(2,1)}) custom-call(bf16[4,4,64,128]{3,2,1,0:T(8,128)(2,1)} %get-tuple-element.19.refs_0_, bf16[4,4,64,128]{3,2,1,0:T(8,128)(2,1)} %collective-permute-done.4.refs_1_, ...), custom_call_target="tpu_custom_call" | custom-call | tf_op jit(solution)/shard_map/pallas_call | solution.py:128
  73.8 5.9 %collective-permute-start.27 = (bf16[2,4,64,128]{3,2,1,0:T(8,128)(2,1)}, bf16[2,4,64,128]{3,2,1,0:T(8,128)(2,1)S(1)}, u32[]{:S(2)}, u32[]{:S(2)}) collective-permute-start(bf16[2,4,64,128]{3,2,1,0:T(8,128)(2,1)} %get-tuple-element.29), channel_id=1, source_target_pairs={{0,16},{8,24},{16,32},{24,40},{32,48},{40,56},{48,64},{56,72},{64,... | collective-permute-start | bytes 393224 | tf_op jit(solution)/shard_map/ppermute | solution.py:32
  79.7 3.5 %collective-permute-done.27.refs_3_ = bf16[2,4,64,128]{3,2,1,0:T(8,128)(2,1)S(1)} collective-permute-done((bf16[2,4,64,128]{3,2,1,0:T(8,128)(2,1)}, bf16[2,4,64,128]{3,2,1,0:T(8,128)(2,1)S(1)}, u32[]{:S(2)}, u32[]{:S(2)}) %collective-permute-start.27) | collective-permute-done | bytes 131104 | tf_op jit(solution)/shard_map/ppermute | solution.py:32
  91.8 4.4 %collective-permute-start.20 = (bf16[8,2,64,128]{3,2,1,0:T(8,128)(2,1)}, bf16[8,2,64,128]{3,2,1,0:T(8,128)(2,1)}, u32[]{:S(2)}, u32[]{:S(2)}) collective-permute-start(bf16[8,2,64,128]{3,2,1,0:T(8,128)(2,1)} %collective-permute-done.11.rest_4_), channel_id=1, source_target_pairs={{0,1},{1,0},{2,3},{3,2},{4,5},{5,4},{6,7},{7,6},{8,9},{9,8},{10,11... | collective-permute-start | bytes 786440 | tf_op jit(solution)/shard_map/ppermute | solution.py:32
  98.3 2.4 %shard_map.50 = (bf16[16,4,64,128]{3,2,1,0:T(8,128)(2,1)}, bf16[8,4,64,128]{3,2,1,0:T(8,128)(2,1)}) custom-call(bf16[4,4,64,128]{3,2,1,0:T(8,128)(2,1)} %get-tuple-element.28.refs_0_, bf16[4,4,64,128]{3,2,1,0:T(8,128)(2,1)} %collective-permute-done.25.refs_1_, bf16[4,4,64,128]{3,2,1,0:T(8,128)(2,1)} %collective-permute-done.26.refs_2_, ...), custom_call_target="tpu_custom_call" | custom-call | tf_op jit(solution)/shard_map/pallas_call | solution.py:128
  101.6 2.2 %collective-permute-start.13 = (bf16[16,2,64,128]{3,2,1,0:T(8,128)(2,1)}, bf16[16,2,64,128]{3,2,1,0:T(8,128)(2,1)S(1)}, u32[]{:S(2)}, u32[]{:S(2)}) collective-permute-start(bf16[16,2,64,128]{3,2,1,0:T(8,128)(2,1)} %get-tuple-element.24), channel_id=1, source_target_pairs={{0,6},{1,7},{2,0},{3,1},{4,2},{5,3},{6,4},{7,5},{8,14},{9,15},{10,... | collective-permute-start | bytes 1572872 | tf_op jit(solution)/shard_map/ppermute | solution.py:32
  105.5 10.1 %collective-permute-done.13.rest_6_ = bf16[16,2,64,128]{3,2,1,0:T(8,128)(2,1)S(1)} collective-permute-done((bf16[16,2,64,128]{3,2,1,0:T(8,128)(2,1)}, bf16[16,2,64,128]{3,2,1,0:T(8,128)(2,1)S(1)}, u32[]{:S(2)}, u32[]{:S(2)}) %collective-permute-start.13) | collective-permute-done | bytes 524320 | tf_op jit(solution)/shard_map/ppermute | solution.py:32
  115.5 12.7 %collective-permute-start.21 = (bf16[8,2,64,128]{3,2,1,0:T(8,128)(2,1)}, bf16[8,2,64,128]{3,2,1,0:T(8,128)(2,1)S(1)}, u32[]{:S(2)}, u32[]{:S(2)}) collective-permute-start(bf16[8,2,64,128]{3,2,1,0:T(8,128)(2,1)} %collective-permute-done.12.rest_5_), channel_id=1, source_target_pairs={{0,1},{1,0},{2,3},{3,2},{4,5},{5,4},{6,7},{7,6},{8,9},{9,8},{10,11... | collective-permute-start | bytes 786440 | tf_op jit(solution)/shard_map/ppermute | solution.py:32
  128.3 10.0 %collective-permute-done.33.rest_1_ = bf16[8,4,64,128]{3,2,1,0:T(8,128)(2,1)S(1)} collective-permute-done((bf16[8,4,64,128]{3,2,1,0:T(8,128)(2,1)}, bf16[8,4,64,128]{3,2,1,0:T(8,128)(2,1)S(1)}, u32[]{:S(2)}, u32[]{:S(2)}) %collective-permute-start.33) | collective-permute-done | bytes 524320 | tf_op jit(solution)/shard_map/ppermute | solution.py:32
  141.9 6.8 %collective-permute-done.30.rest_1_ = bf16[16,4,64,128]{3,2,1,0:T(8,128)(2,1)S(1)} collective-permute-done((bf16[16,4,64,128]{3,2,1,0:T(8,128)(2,1)}, bf16[16,4,64,128]{3,2,1,0:T(8,128)(2,1)S(1)}, u32[]{:S(2)}, u32[]{:S(2)}) %collective-permute-start.30) | collective-permute-done | bytes 1048608 | tf_op jit(solution)/shard_map/ppermute | solution.py:32
  150.0 3.6 %collective-permute-done.9.rest_2_ = bf16[8,4,64,128]{3,2,1,0:T(8,128)(2,1)S(1)} collective-permute-done((bf16[8,4,64,128]{3,2,1,0:T(8,128)(2,1)}, bf16[8,4,64,128]{3,2,1,0:T(8,128)(2,1)S(1)}, u32[]{:S(2)}, u32[]{:S(2)}) %collective-permute-start.9) | collective-permute-done | bytes 524320 | tf_op jit(solution)/shard_map/ppermute | solution.py:32
  156.4 10.0 %collective-permute-done.34.rest_2_ = bf16[8,4,64,128]{3,2,1,0:T(8,128)(2,1)S(1)} collective-permute-done((bf16[8,4,64,128]{3,2,1,0:T(8,128)(2,1)S(1)}, bf16[8,4,64,128]{3,2,1,0:T(8,128)(2,1)S(1)}, u32[]{:S(2)}, u32[]{:S(2)}) %collective-permute-start.34) | collective-permute-done | bytes 524320 | tf_op jit(solution)/shard_map/ppermute | solution.py:32
  168.7 7.2 %shard_map.46.pooled_ref = bf16[400,4096]{1,0:T(8,128)(2,1)S(1)} custom-call(bf16[32,4096]{1,0:T(8,128)(2,1)S(1)} %collective-permute-done.halo_ref, f32[2,4096]{1,0:T(2,128)S(1)} %copy-done.6, bf16[384,4096]{1,0:T(8,128)(2,1)S(1)} %copy-done.1), custom_call_target="tpu_custom_call" | custom-call | tf_op jit(solution)/shard_map/pallas_call | solution.py:361
  177.7 13.7 %shard_map.49 = (f32[384,4096]{1,0:T(8,128)}, bf16[384,4096]{1,0:T(8,128)(2,1)S(1)}) custom-call(bf16[32,4096]{1,0:T(8,128)(2,1)S(1)} %collective-permute-done.halo_ref, bf16[384,4096]{1,0:T(8,128)(2,1)} %stream_ref.1, bf16[400,4096]{1,0:T(8,128)(2,1)} %copy-done.2, f32[2,4096]{1,0:T(2,128)S(1)} %copy-done.5, f32[2,4096]{1,0:T(2,128)S(1)} %copy-done.7, ...), custom_call_target="tpu_custom_call" | custom-call | tf_op jit(solution)/shard_map/pallas_call | solution.py:361
  191.4 2.8 %copy-done = f32[384,4096]{1,0:T(8,128)S(1)} copy-done((f32[384,4096]{1,0:T(8,128)S(1)}, f32[384,4096]{1,0:T(8,128)}, u32[]{:S(2)}) %copy-start) | copy-done | bytes 6291480
  194.2 4.8 %shard_map.51.rest_4_ = bf16[384,4096]{1,0:T(8,128)(2,1)} custom-call(f32[384,4096]{1,0:T(8,128)S(1)} %copy-done, bf16[384,4096]{1,0:T(8,128)(2,1)S(1)} %get-tuple-element.27.pooled_ref, f32[2,4096]{1,0:T(2,128)S(1)} %copy-done.5, bf16[16,4,64,128]{3,2,1,0:T(8,128)(2,1)S(1)} %copy-done.3, bf16[8,4,64,128]{3,2,1,0:T(8,128)(2,1)S(1)} %collective-permute-done.33.rest_1_, ...), custom_call_target="tpu_custom_call" | custom-call | tf_op jit(solution)/shard_map/pallas_call | solution.py:340
  199.0 4.7 %shard_map.52 = bf16[384,4096]{1,0:T(8,128)(2,1)} custom-call(f32[384,4096]{1,0:T(8,128)S(1)} %copy-done, bf16[384,4096]{1,0:T(8,128)(2,1)S(1)} %get-tuple-element.27.pooled_ref, f32[2,4096]{1,0:T(2,128)S(1)} %copy-done.5, bf16[16,4,64,128]{3,2,1,0:T(8,128)(2,1)S(1)} %collective-permute-done.29.rest_0_, ...), custom_call_target="tpu_custom_call", output_to_operand_aliasing={{}: (7, {})} | custom-call | tf_op jit(solution)/shard_map/pallas_call | solution.py:340
  (86 shorter events, 35.3 us)
Async XLA Ops:
  0.0 26.9 %collective-permute-start.1 = (bf16[2,4,64,128]{3,2,1,0:T(8,128)(2,1)}, bf16[2,4,64,128]{3,2,1,0:T(8,128)(2,1)S(1)}, u32[]{:S(2)}, u32[]{:S(2)}) collective-permute-start(bf16[2,4,64,128]{3,2,1,0:T(8,128)(2,1)} %refs_1_.1), channel_id=1, source_target_pairs={{0,96},{8,104},{16,112},{24,120},{32,0},{40,8},{48,16},{56,24},{64... | collective-permute-start | bytes 393224 | tf_op jit(solution)/shard_map/ppermute | solution.py:32
  21.7 25.9 %collective-permute-start.3 = (bf16[2,4,64,128]{3,2,1,0:T(8,128)(2,1)}, bf16[2,4,64,128]{3,2,1,0:T(8,128)(2,1)S(1)}, u32[]{:S(2)}, u32[]{:S(2)}) collective-permute-start(bf16[2,4,64,128]{3,2,1,0:T(8,128)(2,1)} %refs_1_.1), channel_id=1, source_target_pairs={{0,64},{8,72},{16,80},{24,88},{32,96},{40,104},{48,112},{56,120},{... | collective-permute-start | bytes 393224 | tf_op jit(solution)/shard_map/ppermute | solution.py:32
  50.4 15.1 %collective-permute-start.4 = (bf16[4,4,64,128]{3,2,1,0:T(8,128)(2,1)}, bf16[4,4,64,128]{3,2,1,0:T(8,128)(2,1)}, u32[]{:S(2)}, u32[]{:S(2)}) collective-permute-start(bf16[4,4,64,128]{3,2,1,0:T(8,128)(2,1)} %get-tuple-element.19.refs_0_), channel_id=1, source_target_pairs={{0,8},{8,16},{16,24},{24,32},{32,40},{40,48},{48,56},{56,64},{64,7... | collective-permute-start | bytes 786440 | tf_op jit(solution)/shard_map/ppermute | solution.py:32
  50.4 15.1 %collective-permute-start.5 = (bf16[4,4,64,128]{3,2,1,0:T(8,128)(2,1)}, bf16[4,4,64,128]{3,2,1,0:T(8,128)(2,1)}, u32[]{:S(2)}, u32[]{:S(2)}) collective-permute-start(bf16[4,4,64,128]{3,2,1,0:T(8,128)(2,1)} %get-tuple-element.19.refs_0_), channel_id=1, source_target_pairs={{0,120},{8,0},{16,8},{24,16},{32,24},{40,32},{48,40},{56,48},{64,5... | collective-permute-start | bytes 786440 | tf_op jit(solution)/shard_map/ppermute | solution.py:32
  58.3 21.4 %collective-permute-start = (bf16[32,4096]{1,0:T(8,128)(2,1)}, bf16[32,4096]{1,0:T(8,128)(2,1)S(1)}, u32[]{:S(2)}, u32[]{:S(2)}) collective-permute-start(bf16[32,4096]{1,0:T(8,128)(2,1)} %slice.3), channel_id=1, source_target_pairs={{0,1},{1,2},{2,3},{3,4},{4,5},{5,6},{6,7},{7,8},{8,9},{9,10},{10,1... | collective-permute-start | bytes 786440 | tf_op jit(solution)/shard_map/ppermute | solution.py:375
  68.8 17.1 %collective-permute-start.11 = (bf16[8,2,64,128]{3,2,1,0:T(8,128)(2,1)}, bf16[8,2,64,128]{3,2,1,0:T(8,128)(2,1)}, u32[]{:S(2)}, u32[]{:S(2)}) collective-permute-start(bf16[8,2,64,128]{3,2,1,0:T(8,128)(2,1)} %get-tuple-element.25), channel_id=1, source_target_pairs={{0,2},{1,3},{2,4},{3,5},{4,6},{5,7},{6,0},{7,1},{8,10},{9,11},{10,... | collective-permute-start | bytes 786440 | tf_op jit(solution)/shard_map/ppermute | solution.py:32
  70.7 17.3 %collective-permute-start.14 = (bf16[8,2,64,128]{3,2,1,0:T(8,128)(2,1)}, bf16[8,2,64,128]{3,2,1,0:T(8,128)(2,1)}, u32[]{:S(2)}, u32[]{:S(2)}) collective-permute-start(bf16[8,2,64,128]{3,2,1,0:T(8,128)(2,1)} %get-tuple-element.25), channel_id=1, source_target_pairs={{0,6},{1,7},{2,0},{3,1},{4,2},{5,3},{6,4},{7,5},{8,14},{9,15},{10,... | collective-permute-start | bytes 786440 | tf_op jit(solution)/shard_map/ppermute | solution.py:32
  72.2 28.9 %collective-permute-start.8 = (bf16[8,4,64,128]{3,2,1,0:T(8,128)(2,1)}, bf16[8,4,64,128]{3,2,1,0:T(8,128)(2,1)}, u32[]{:S(2)}, u32[]{:S(2)}) collective-permute-start(bf16[8,4,64,128]{3,2,1,0:T(8,128)(2,1)} %get-tuple-element.23), channel_id=1, source_target_pairs={{0,4},{1,5},{2,6},{3,7},{4,0},{5,1},{6,2},{7,3},{8,12},{9,13},{10,... | collective-permute-start | bytes 1572872 | tf_op jit(solution)/shard_map/ppermute | solution.py:32
  90.2 14.0 %collective-permute-start.10 = (bf16[16,2,64,128]{3,2,1,0:T(8,128)(2,1)}, bf16[16,2,64,128]{3,2,1,0:T(8,128)(2,1)}, u32[]{:S(2)}, u32[]{:S(2)}) collective-permute-start(bf16[16,2,64,128]{3,2,1,0:T(8,128)(2,1)} %get-tuple-element.24), channel_id=1, source_target_pairs={{0,2},{1,3},{2,4},{3,5},{4,6},{5,7},{6,0},{7,1},{8,10},{9,11},{10,... | collective-permute-start | bytes 1572872 | tf_op jit(solution)/shard_map/ppermute | solution.py:32
  100.8 40.6 %collective-permute-start.16 = (bf16[16,4,64,128]{3,2,1,0:T(8,128)(2,1)}, bf16[16,4,64,128]{3,2,1,0:T(8,128)(2,1)S(1)}, u32[]{:S(2)}, u32[]{:S(2)}) collective-permute-start(bf16[16,4,64,128]{3,2,1,0:T(8,128)(2,1)} %get-tuple-element.22.rest_0_), channel_id=1, source_target_pairs={{0,1},{1,0},{2,3},{3,2},{4,5},{5,4},{6,7},{7,6},{8,9},{9,8},{10,11... | collective-permute-start | bytes 3145736 | tf_op jit(solution)/shard_map/ppermute | solution.py:32
  101.1 40.4 %collective-permute-start.29 = (bf16[16,4,64,128]{3,2,1,0:T(8,128)(2,1)}, bf16[16,4,64,128]{3,2,1,0:T(8,128)(2,1)S(1)}, u32[]{:S(2)}, u32[]{:S(2)}) collective-permute-start(bf16[16,4,64,128]{3,2,1,0:T(8,128)(2,1)} %get-tuple-element.31.rest_0_), channel_id=1, source_target_pairs={{0,2},{1,3},{2,4},{3,5},{4,6},{5,7},{6,0},{7,1},{8,10},{9,11},{10,... | collective-permute-start | bytes 3145736 | tf_op jit(solution)/shard_map/ppermute | solution.py:32
  101.6 13.9 %collective-permute-start.13 = (bf16[16,2,64,128]{3,2,1,0:T(8,128)(2,1)}, bf16[16,2,64,128]{3,2,1,0:T(8,128)(2,1)S(1)}, u32[]{:S(2)}, u32[]{:S(2)}) collective-permute-start(bf16[16,2,64,128]{3,2,1,0:T(8,128)(2,1)} %get-tuple-element.24), channel_id=1, source_target_pairs={{0,6},{1,7},{2,0},{3,1},{4,2},{5,3},{6,4},{7,5},{8,14},{9,15},{10,... | collective-permute-start | bytes 1572872 | tf_op jit(solution)/shard_map/ppermute | solution.py:32
  103.8 34.4 %collective-permute-start.33 = (bf16[8,4,64,128]{3,2,1,0:T(8,128)(2,1)}, bf16[8,4,64,128]{3,2,1,0:T(8,128)(2,1)S(1)}, u32[]{:S(2)}, u32[]{:S(2)}) collective-permute-start(bf16[8,4,64,128]{3,2,1,0:T(8,128)(2,1)} %get-tuple-element.32), channel_id=1, source_target_pairs={{0,4},{1,5},{2,6},{3,7},{4,0},{5,1},{6,2},{7,3},{8,12},{9,13},{10,... | collective-permute-start | bytes 1572872 | tf_op jit(solution)/shard_map/ppermute | solution.py:32
  104.2 44.5 %collective-permute-start.30 = (bf16[16,4,64,128]{3,2,1,0:T(8,128)(2,1)}, bf16[16,4,64,128]{3,2,1,0:T(8,128)(2,1)S(1)}, u32[]{:S(2)}, u32[]{:S(2)}) collective-permute-start(bf16[16,4,64,128]{3,2,1,0:T(8,128)(2,1)} %get-tuple-element.31.rest_0_), channel_id=1, source_target_pairs={{0,6},{1,7},{2,0},{3,1},{4,2},{5,3},{6,4},{7,5},{8,14},{9,15},{10,... | collective-permute-start | bytes 3145736 | tf_op jit(solution)/shard_map/ppermute | solution.py:32
  115.5 23.6 %collective-permute-start.21 = (bf16[8,2,64,128]{3,2,1,0:T(8,128)(2,1)}, bf16[8,2,64,128]{3,2,1,0:T(8,128)(2,1)S(1)}, u32[]{:S(2)}, u32[]{:S(2)}) collective-permute-start(bf16[8,2,64,128]{3,2,1,0:T(8,128)(2,1)} %collective-permute-done.12.rest_5_), channel_id=1, source_target_pairs={{0,1},{1,0},{2,3},{3,2},{4,5},{5,4},{6,7},{7,6},{8,9},{9,8},{10,11... | collective-permute-start | bytes 786440 | tf_op jit(solution)/shard_map/ppermute | solution.py:32
  139.2 14.4 %collective-permute-start.9 = (bf16[8,4,64,128]{3,2,1,0:T(8,128)(2,1)}, bf16[8,4,64,128]{3,2,1,0:T(8,128)(2,1)S(1)}, u32[]{:S(2)}, u32[]{:S(2)}) collective-permute-start(bf16[8,4,64,128]{3,2,1,0:T(8,128)(2,1)} %collective-permute-done.8.rest_1_), channel_id=1, source_target_pairs={{0,128},{128,0},{1,129},{129,1},{2,130},{130,2},{3,131},{131,3},{4... | collective-permute-start | bytes 1572872 | tf_op jit(solution)/shard_map/ppermute | solution.py:32
  141.1 13.7 %collective-permute-start.17 = (bf16[8,4,64,128]{3,2,1,0:T(8,128)(2,1)}, bf16[8,4,64,128]{3,2,1,0:T(8,128)(2,1)S(1)}, u32[]{:S(2)}, u32[]{:S(2)}) collective-permute-start(bf16[8,4,64,128]{3,2,1,0:T(8,128)(2,1)} %collective-permute-done.8.rest_1_), channel_id=1, source_target_pairs={{0,1},{1,0},{2,3},{3,2},{4,5},{5,4},{6,7},{7,6},{8,9},{9,8},{10,11... | collective-permute-start | bytes 1572872 | tf_op jit(solution)/shard_map/ppermute | solution.py:32
  141.4 14.5 %collective-permute-start.19 = (bf16[16,2,64,128]{3,2,1,0:T(8,128)(2,1)}, bf16[16,2,64,128]{3,2,1,0:T(8,128)(2,1)S(1)}, u32[]{:S(2)}, u32[]{:S(2)}) collective-permute-start(bf16[16,2,64,128]{3,2,1,0:T(8,128)(2,1)} %collective-permute-done.10.rest_3_), channel_id=1, source_target_pairs={{0,1},{1,0},{2,3},{3,2},{4,5},{5,4},{6,7},{7,6},{8,9},{9,8},{10,11... | collective-permute-start | bytes 1572872 | tf_op jit(solution)/shard_map/ppermute | solution.py:32
  141.6 14.4 %collective-permute-start.22 = (bf16[16,2,64,128]{3,2,1,0:T(8,128)(2,1)S(1)}, bf16[16,2,64,128]{3,2,1,0:T(8,128)(2,1)S(1)}, u32[]{:S(2)}, u32[]{:S(2)}) collective-permute-start(bf16[16,2,64,128]{3,2,1,0:T(8,128)(2,1)S(1)} %collective-permute-done.13.rest_6_), channel_id=1, source_target_pairs={{0,1},{1,0},{2,3},{3,2},{4,5},{5,4},{6,7},{7,6},{8,9},{9,8},{10,11... | collective-permute-start | bytes 1572872 | tf_op jit(solution)/shard_map/ppermute | solution.py:32
  148.7 42.7 %collective-permute-start.35 = (bf16[16,4,64,128]{3,2,1,0:T(8,128)(2,1)}, bf16[16,4,64,128]{3,2,1,0:T(8,128)(2,1)S(1)}, u32[]{:S(2)}, u32[]{:S(2)}) collective-permute-start(bf16[16,4,64,128]{3,2,1,0:T(8,128)(2,1)} %get-tuple-element.31.rest_0_), channel_id=1, source_target_pairs={{0,1},{1,0},{2,3},{3,2},{4,5},{5,4},{6,7},{7,6},{8,9},{9,8},{10,11... | collective-permute-start | bytes 3145736 | tf_op jit(solution)/shard_map/ppermute | solution.py:32
  155.9 43.1 %collective-permute-start.31 = (bf16[16,4,64,128]{3,2,1,0:T(8,128)(2,1)S(1)}, bf16[16,4,64,128]{3,2,1,0:T(8,128)(2,1)S(1)}, u32[]{:S(2)}, u32[]{:S(2)}) collective-permute-start(bf16[16,4,64,128]{3,2,1,0:T(8,128)(2,1)S(1)} %collective-permute-done.29.rest_0_), channel_id=1, source_target_pairs={{0,1},{1,0},{2,3},{3,2},{4,5},{5,4},{6,7},{7,6},{8,9},{9,8},{10,11... | collective-permute-start | bytes 3145736 | tf_op jit(solution)/shard_map/ppermute | solution.py:32
  156.0 43.0 %collective-permute-start.32 = (bf16[16,4,64,128]{3,2,1,0:T(8,128)(2,1)S(1)}, bf16[16,4,64,128]{3,2,1,0:T(8,128)(2,1)S(1)}, u32[]{:S(2)}, u32[]{:S(2)}) collective-permute-start(bf16[16,4,64,128]{3,2,1,0:T(8,128)(2,1)S(1)} %collective-permute-done.30.rest_1_), channel_id=1, source_target_pairs={{0,1},{1,0},{2,3},{3,2},{4,5},{5,4},{6,7},{7,6},{8,9},{9,8},{10,11... | collective-permute-start | bytes 3145736 | tf_op jit(solution)/shard_map/ppermute | solution.py:32
  166.5 24.9 %collective-permute-start.36 = (bf16[8,4,64,128]{3,2,1,0:T(8,128)(2,1)S(1)}, bf16[8,4,64,128]{3,2,1,0:T(8,128)(2,1)S(1)}, u32[]{:S(2)}, u32[]{:S(2)}) collective-permute-start(bf16[8,4,64,128]{3,2,1,0:T(8,128)(2,1)S(1)} %collective-permute-done.33.rest_1_), channel_id=1, source_target_pairs={{0,1},{1,0},{2,3},{3,2},{4,5},{5,4},{6,7},{7,6},{8,9},{9,8},{10,11... | collective-permute-start | bytes 1572872 | tf_op jit(solution)/shard_map/ppermute | solution.py:32
  167.9 23.5 %collective-permute-start.37 = (bf16[8,4,64,128]{3,2,1,0:T(8,128)(2,1)S(1)}, bf16[8,4,64,128]{3,2,1,0:T(8,128)(2,1)S(1)}, u32[]{:S(2)}, u32[]{:S(2)}) collective-permute-start(bf16[8,4,64,128]{3,2,1,0:T(8,128)(2,1)S(1)} %collective-permute-done.34.rest_2_), channel_id=1, source_target_pairs={{0,1},{1,0},{2,3},{3,2},{4,5},{5,4},{6,7},{7,6},{8,9},{9,8},{10,11... | collective-permute-start | bytes 1572872 | tf_op jit(solution)/shard_map/ppermute | solution.py:32
  (27 other events, 526.2 us)
